TPU v7x, 512 devices: a whole 4x4x16 slice. The times are simulated.
512 devices in a mesh: fs: 64 (over z, y), tp: 8 (over x, core).
Axes of the slice: x: 4, y: 4, z: 16, core: 2. Of those that a mesh axis runs over, the one named last changes fastest.
Arguments:
- residual_in: bfloat16 [16384, 2048], P(('fs', 'tp')), may hold values from -6 to 6
- gain_first: float32 [2048], replicated, may hold values from 0.1 to 1.9
- gain_mixer: float32 [2048], replicated, may hold values from 0.1 to 1.9
- gain_second: float32 [2048], replicated, may hold values from 0.1 to 1.9
- gate_weight: float32 [2048, 6144], P('fs', 'tp'), may hold values from -0.125 to 0.125
- gate_scale: float32 [6144], P('tp'), may hold values from 0.3 to 3
- up_weight: float32 [2048, 6144], P('fs', 'tp'), may hold values from -0.125 to 0.125
- up_scale: float32 [6144], P('tp'), may hold values from 0.3 to 3
- down_weight: float32 [6144, 2048], P('tp', 'fs'), may hold values from -0.078125 to 0.078125
- down_scale: float32 [2048], P('fs'), may hold values from 0.3 to 3
- query_weight: float32 [2048, 2048], P('fs', 'tp'), may hold values from -0.125 to 0.125
- query_scale: float32 [2048], P('tp'), may hold values from 0.3 to 3
- key_weight: float32 [2048, 2048], P('fs', 'tp'), may hold values from -0.125 to 0.125
- key_scale: float32 [2048], P('tp'), may hold values from 0.3 to 3
- value_weight: float32 [2048, 2048], P('fs', 'tp'), may hold values from -0.125 to 0.125
- value_scale: float32 [2048], P('tp'), may hold values from 0.3 to 3
- output_weight: float32 [2048, 2048], P('tp', 'fs'), may hold values from -0.125 to 0.125
- output_scale: float32 [2048], P('fs'), may hold values from 0.3 to 3
Outputs:
- residual_out: bfloat16 [16384, 2048], P(('fs', 'tp'))
All inputs are finite; a program needn't handle non-finite values.
Results may differ from a plain program's by a relative error of at most 0.028.
Values may be sent and summed in bfloat16 or wider, within the bound.
No kernel may reach another device: no remote copies, remote signals or barrier semaphores. Data moves between devices by JAX's collectives and lax.ppermute only.
A program may use at most 64 MiB of HBM per device.

v0:
```python
import jax
import jax.numpy as jnp
from jax import lax
from jax.sharding import Mesh
from jax.sharding import PartitionSpec as P

HEADS = 8
HEAD_DIM = 256
BLOCK = 64
FS = ("fs_0", "fs_1")
FS_TP = ("fs_0", "fs_1", "tp")
EPSILON = 1e-06
HEAD_FLOOR = 0.25
ROTARY_BASE = 10000.0
HIGHEST = lax.Precision.HIGHEST


def sent_to_all(x, axis):
    peers = lax.axis_size(axis)
    return lax.all_to_all(jnp.broadcast_to(x[None], (peers, *x.shape)), axis, 0, 0, tiled=True)


def in_order(pieces, dim):
    dims = list(pieces.shape[1:])
    dims[dim] *= pieces.shape[0]
    return jnp.moveaxis(pieces, 0, dim).reshape(dims)


def collect(x, axis, dim):
    pieces = sent_to_all(x, axis)
    return in_order(pieces, dim)


def split_up(x, dim, peers):
    dims = x.shape
    pieces = x.reshape(*dims[:dim], peers, dims[dim] // peers, *dims[dim + 1 :])
    return jnp.moveaxis(pieces, dim, 0)


def sent_and_summed(x, axis, dim):
    pieces = split_up(x, dim, lax.axis_size(axis))
    arrived = lax.all_to_all(pieces, axis, split_axis=0, concat_axis=0, tiled=True)
    return arrived.astype(jnp.float32).sum(axis=0)


def gather_turned(arrays, axis, dims):
    turned = [jnp.moveaxis(a, dim, 0) for a, dim in zip(arrays, dims)]
    widths = [t[0].size for t in turned]
    both = jnp.concatenate([t.reshape(-1, w) for t, w in zip(turned, widths)], axis=1)
    whole = lax.all_gather(both, axis, axis=0, tiled=True)
    pieces = jnp.split(whole, [sum(widths[:k]) for k in range(1, len(widths))], axis=1)
    return tuple(
        (
            jnp.moveaxis(b.reshape(-1, *t.shape[1:]), 0, dim)
            for b, t, dim in zip(pieces, turned, dims)
        )
    )


def side_by_side(arrays, axis, dim, along):
    both = jnp.concatenate(arrays, axis=along)
    whole, at, done = (lax.all_gather(both, axis, axis=dim, tiled=True), 0, [])
    for a in arrays:
        done.append(lax.slice_in_dim(whole, at, at + a.shape[along], axis=along))
        at += a.shape[along]
    return tuple(done)


def gather_axes(x, axes, dim):
    whole = x
    for number in range(len(axes) - 1, -1, -1):
        whole = lax.all_gather(whole, axes[number], axis=dim, tiled=True)
    return whole


def normalize(sequence_rows, gain_vector):
    values = sequence_rows.astype(jnp.float32)
    scaled = values * lax.rsqrt(jnp.mean(values * values, axis=-1, keepdims=True) + EPSILON)
    return (scaled * gain_vector).astype(jnp.bfloat16)


def collect_rows(sequence_rows, gain_vector):
    return collect(normalize(sequence_rows, gain_vector), "tp", 0)


def return_rows(inputs, weight, factor):
    term = jnp.dot(inputs, weight, preferred_element_type=jnp.float32) * factor
    return sent_and_summed(
        lax.optimization_barrier(term.astype(jnp.bfloat16))
        .astype(jnp.float32)
        .astype(jnp.bfloat16),
        "tp",
        0,
    )


def head_rates(first_head, head_count, length):
    head_number = (first_head + jnp.arange(head_count)).astype(jnp.float32)
    return jnp.exp(jnp.log(1.0 / 16.0) + head_number / (HEADS - 1) * jnp.log(4.0 / length))


def rotate(values, positions):
    half_width = values.shape[-1] // 2
    frequency = ROTARY_BASE ** (-jnp.arange(half_width, dtype=jnp.float32) * 2.0 / values.shape[-1])
    angles = positions[:, None] * frequency[None, :]
    cosine = jnp.cos(angles)[:, None, :]
    sine_value = jnp.sin(angles)[:, None, :]
    front_half = values[..., :half_width]
    back_half = values[..., half_width:]
    return jnp.concatenate(
        [
            front_half * cosine - back_half * sine_value,
            back_half * cosine + front_half * sine_value,
        ],
        axis=-1,
    )


def retention(query_pre, key_pre, value_pre, decay_rates):
    length, head_count, head_width = query_pre.shape
    positions = jnp.arange(length, dtype=jnp.float32)
    query_rot = rotate(query_pre, positions).astype(jnp.bfloat16)
    key_rot = rotate(key_pre, positions).astype(jnp.bfloat16)
    value_low = value_pre.astype(jnp.bfloat16)
    blocks = length // BLOCK
    inside = jnp.arange(BLOCK, dtype=jnp.float32)
    distance = inside[:, None] - inside[None, :]
    within = jnp.where(
        distance >= 0, jnp.exp(-decay_rates[:, None, None] * jnp.maximum(distance, 0.0)), 0.0
    ) * head_width ** (-0.5)
    query_blocks = query_rot.reshape(blocks, BLOCK, head_count, head_width)
    key_blocks = key_rot.reshape(blocks, BLOCK, head_count, head_width)
    value_blocks = value_low.reshape(blocks, BLOCK, head_count, head_width)
    scores = jnp.einsum(
        "nihe,njhe->nhij", query_blocks, key_blocks, preferred_element_type=jnp.float32
    )
    weights = (scores * within[None]).astype(jnp.bfloat16)
    inner_part = jnp.einsum(
        "nhij,njhe->nihe", weights, value_blocks, preferred_element_type=jnp.float32
    )
    fading = jnp.exp(-decay_rates[None, :] * (BLOCK - 1.0 - inside[:, None])) * head_width ** (-0.5)
    key_faded = key_blocks.astype(jnp.float32) * fading[None, :, :, None]
    updates = jnp.einsum(
        "njhd,njhe->nhde", key_faded, value_blocks.astype(jnp.float32), precision=HIGHEST
    )
    block_decay = jnp.exp(-decay_rates * BLOCK)

    def advance(memory_state, update):
        return (memory_state * block_decay[:, None, None] + update, memory_state)

    _, before = lax.scan(
        advance, jnp.zeros((head_count, head_width, head_width), jnp.float32), updates
    )
    rising = jnp.exp(-decay_rates[None, :] * (inside[:, None] + 1.0))
    queried = query_blocks.astype(jnp.float32) * rising[None, :, :, None]
    carried_part = jnp.einsum("nihd,nhde->nihe", queried, before, precision=HIGHEST)
    combined = (inner_part + carried_part).reshape(length, head_count, head_width)
    normed = combined * lax.rsqrt(
        jnp.maximum(jnp.mean(combined * combined, axis=-1, keepdims=True), HEAD_FLOOR)
    )
    return normed.astype(jnp.bfloat16).reshape(length, head_count * head_width)


def body(
    residual_in,
    gain_first,
    gain_mixer,
    gain_second,
    gate_weight,
    gate_scale,
    up_weight,
    up_scale,
    down_weight,
    down_scale,
    query_weight,
    query_scale,
    key_weight,
    key_scale,
    value_weight,
    value_scale,
    output_weight,
    output_scale,
):
    gate_part = gate_weight.astype(jnp.bfloat16)
    up_part = up_weight.astype(jnp.bfloat16)
    down_factor, output_factor = gather_turned((down_scale, output_scale), FS, (0, 0))
    first_input = collect_rows(residual_in, gain_first)
    gate_full, up_full = side_by_side((gate_part, up_part), FS, 0, 1)
    gate_pre = jnp.dot(first_input, gate_full, preferred_element_type=jnp.float32)
    up_pre = jnp.dot(first_input, up_full, preferred_element_type=jnp.float32)
    down_full = gather_axes(down_weight.astype(jnp.bfloat16), FS, 1)
    hidden_first = (jax.nn.silu(gate_pre * gate_scale) * (up_pre * up_scale)).astype(jnp.bfloat16)
    mlp_first = return_rows(hidden_first, down_full, down_factor)
    middle = (residual_in.astype(jnp.float32) + 0.5 * mlp_first).astype(jnp.bfloat16)
    mixer_input = collect_rows(middle, gain_mixer)
    local_width = query_weight.shape[1]
    projections = (
        query_weight.astype(jnp.bfloat16),
        key_weight.astype(jnp.bfloat16),
        value_weight.astype(jnp.bfloat16),
    )
    pieces = side_by_side((projections[0], projections[1], projections[2]), FS, 0, 1)
    query_pre, key_pre, value_pre = tuple(
        (
            jnp.dot(mixer_input, pieces[member], preferred_element_type=jnp.float32)
            for member in range(3)
        )
    )
    output_full = gather_axes(output_weight.astype(jnp.bfloat16), FS, 1)
    length = mixer_input.shape[0]
    heads_local = local_width // HEAD_DIM
    decay_rates = head_rates(lax.axis_index("tp") * heads_local, heads_local, length)
    mixed = retention(
        (query_pre * query_scale).reshape(length, heads_local, HEAD_DIM),
        (key_pre * key_scale).reshape(length, heads_local, HEAD_DIM),
        (value_pre * value_scale).reshape(length, heads_local, HEAD_DIM),
        decay_rates,
    )
    mixer_out = return_rows(mixed, output_full, output_factor)
    second = (middle.astype(jnp.float32) + mixer_out).astype(jnp.bfloat16)
    last_input = collect_rows(second, gain_second)
    gate_last = jnp.dot(last_input, gate_full, preferred_element_type=jnp.float32) * gate_scale
    up_last = jnp.dot(last_input, up_full, preferred_element_type=jnp.float32) * up_scale
    hidden_second = (jax.nn.silu(gate_last) * up_last).astype(jnp.bfloat16)
    mlp_second = return_rows(hidden_second, down_full, down_factor)
    return (second.astype(jnp.float32) + 0.5 * mlp_second).astype(jnp.bfloat16)


def solution(mesh):
    split = Mesh(mesh.devices.reshape(16, 4, mesh.shape["tp"]), ("fs_0", "fs_1", "tp"))
    in_specs = (
        P(FS_TP, None),
        P(),
        P(),
        P(),
        P(FS, "tp"),
        P("tp"),
        P(FS, "tp"),
        P("tp"),
        P("tp", FS),
        P(FS),
        P(FS, "tp"),
        P("tp"),
        P(FS, "tp"),
        P("tp"),
        P(FS, "tp"),
        P("tp"),
        P("tp", FS),
        P(FS),
    )
    out_specs = P(FS_TP, None)
    return jax.shard_map(body, mesh=split, in_specs=in_specs, out_specs=out_specs, check_vma=False)
```

profile of v0, /device:TPU:1, one launch (start us, length us, event | category | flops | bytes accessed | tf_op | source)
XLA Modules:
  0.0 524.1 jit_solution(4226606983639578589)
XLA Ops:
  10.0 11.3 %all_gather.22 = bf16[768,128]{0,1:T(8,128)(2,1)} all-gather(bf16[768,32]{0,1:T(8,128)(2,1)S(1)} %convert_element_type.133), channel_id=1, replica_groups=mesh['fs_0'=16,'fs_1'=4,'tp'=8] {'fs_1'}, dimensions={1}, use_global_device_ids=true | all-gather | bytes 245760 | tf_op jit(solution)/shard_map/all_gather | solution.py:72
  24.3 1.0 fusion.58
  26.4 1.2 broadcast_in_dim.15
  27.6 11.8 %all-to-all-start = ((bf16[8,32,2048]{2,1,0:T(8,128)(2,1)}), bf16[8,32,2048]{2,1,0:T(8,128)(2,1)S(1)}, u32[]{:S(2)}, u32[]{:S(2)}) async-start(bf16[8,32,2048]{2,1,0:T(8,128)(2,1)} %broadcast_in_dim.15), calls=%async_computation | async-start | bytes 2097152 | tf_op jit(solution)/shard_map/all_to_all | solution.py:20
  39.4 72.2 %all-gather = f32[64,32,2]{1,2,0:T(2,128)S(1)} all-gather(f32[1,32,2]{1,2,0:T(2,128)S(1)} %maximum_bitcast_fusion), channel_id=1, replica_groups=mesh['fs_0'=16,'fs_1'=4,'tp'=8] {'fs_0','fs_1'}, dimensions={0}, use_global_device_ids=true | all-gather | bytes 16640 | tf_op jit(solution)/shard_map/all_gather | solution.py:50
  111.8 46.5 %all-gather.6.cloned.1.call-done = bf16[2048,1536]{1,0:T(8,128)(2,1)} async-done(((bf16[32,1536]{1,0:T(8,128)(2,1)}), bf16[2048,1536]{1,0:T(8,128)(2,1)}) %all-gather.6.cloned.1.call-update) | async-done | bytes 6291472 | tf_op jit(solution)/shard_map/all_gather | solution.py:62
  158.3 2.9 fusion.11
  161.2 69.2 %all-gather.8.cloned.1.call-done = bf16[768,2048]{0,1:T(8,128)(2,1)} async-done(((bf16[768,128]{0,1:T(8,128)(2,1)}), bf16[768,2048]{0,1:T(8,128)(2,1)}) %all-gather.8.cloned.1.call-update) | async-done | bytes 3145744 | tf_op jit(solution)/shard_map/all_gather | solution.py:72
  230.4 5.0 fusion.8
  235.4 28.7 %all_to_all.30 = bf16[8,32,2048]{2,1,0:T(8,128)(2,1)S(1)} all-to-all(bf16[8,32,2048]{2,1,0:T(8,128)(2,1)S(1)} %bitcast.75), channel_id=1, replica_groups=mesh['fs_0'=16,'fs_1'=4,'tp'=8] {'tp'}, dimensions={0} | all-to-all | bytes 2097152 | tf_op jit(solution)/shard_map/all_to_all | solution.py:42
  264.6 1.1 broadcast_in_dim.16
  265.7 4.5 all-to-all-start.2
  270.2 10.6 %all_gather.26 = bf16[256,128]{0,1:T(8,128)(2,1)} all-gather(bf16[256,32]{0,1:T(8,128)(2,1)S(1)} %convert_element_type.148), channel_id=1, replica_groups=mesh['fs_0'=16,'fs_1'=4,'tp'=8] {'fs_1'}, dimensions={1}, use_global_device_ids=true | all-gather | bytes 81920 | tf_op jit(solution)/shard_map/all_gather | solution.py:72
  281.0 92.5 %all-gather.10.cloned.1.call-done = bf16[2048,768]{1,0:T(8,128)(2,1)} async-done(((bf16[32,768]{1,0:T(8,128)(2,1)}), bf16[2048,768]{1,0:T(8,128)(2,1)}) %all-gather.10.cloned.1.call-update) | async-done | bytes 3145744 | tf_op jit(solution)/shard_map/all_gather | solution.py:62
  373.5 1.7 fusion.35
  375.2 1.7 fusion.36
  377.5 1.7 fusion.37
  381.8 58.0 %all-gather.12.cloned.1.call-done = bf16[256,2048]{0,1:T(8,128)(2,1)} async-done(((bf16[256,128]{0,1:T(8,128)(2,1)}), bf16[256,2048]{0,1:T(8,128)(2,1)}) %all-gather.12.cloned.1.call-update) | async-done | bytes 1048592 | tf_op jit(solution)/shard_map/all_gather | solution.py:72
  439.8 1.7 fusion.10
  441.5 30.0 %all_to_all.31 = bf16[8,32,2048]{2,1,0:T(8,128)(2,1)S(1)} all-to-all(bf16[8,32,2048]{2,1,0:T(8,128)(2,1)S(1)} %bitcast.66), channel_id=1, replica_groups=mesh['fs_0'=16,'fs_1'=4,'tp'=8] {'tp'}, dimensions={0} | all-to-all | bytes 2097152 | tf_op jit(solution)/shard_map/all_to_all | solution.py:42
  472.0 18.4 %all_to_all.32 = bf16[8,32,2048]{2,1,0:T(8,128)(2,1)S(1)} all-to-all(bf16[8,32,2048]{2,1,0:T(8,128)(2,1)S(1)} %broadcast_in_dim.19), channel_id=1, replica_groups=mesh['fs_0'=16,'fs_1'=4,'tp'=8] {'tp'}, dimensions={0} | all-to-all | bytes 2097152 | tf_op jit(solution)/shard_map/all_to_all | solution.py:20
  490.4 2.9 fusion.14
  493.3 5.0 fusion.9
  498.4 18.4 %all_to_all.33 = bf16[8,32,2048]{2,1,0:T(8,128)(2,1)S(1)} all-to-all(bf16[8,32,2048]{2,1,0:T(8,128)(2,1)S(1)} %bitcast.74), channel_id=1, replica_groups=mesh['fs_0'=16,'fs_1'=4,'tp'=8] {'tp'}, dimensions={0} | all-to-all | bytes 2097152 | tf_op jit(solution)/shard_map/all_to_all | solution.py:42
  (80 shorter events, 13.1 us)
Async XLA Ops:
  6.5 32.9 %copy-start.5 = (f32[32]{0:T(128)S(1)}, f32[32]{0:T(128)}, u32[]{:S(2)}) copy-start(f32[32]{0:T(128)} %param.29) | copy-start | bytes 388
  6.5 32.9 %copy-start.4 = (f32[32]{0:T(128)S(1)}, f32[32]{0:T(128)}, u32[]{:S(2)}) copy-start(f32[32]{0:T(128)} %param.37) | copy-start | bytes 388
  6.5 151.7 %copy-start.6 = (f32[768]{0:T(1024)S(1)}, f32[768]{0:T(1024)}, u32[]{:S(2)}) copy-start(f32[768]{0:T(1024)} %param.25) | copy-start | bytes 9220
  6.5 151.7 %all-gather.6.cloned.1.call-start = ((), (), s32[]{:S(2)}) async-start(), calls=%async_computation.6 | async-start | bytes 6389760 | tf_op jit(solution)/shard_map/all_gather | solution.py:62
  9.1 221.3 %all-gather.8.cloned.1.call-start = ((), (), s32[]{:S(2)}) async-start(), calls=%async_computation.7 | async-start | bytes 3342336 | tf_op jit(solution)/shard_map/all_gather | solution.py:72
  21.3 352.2 %all-gather.10.cloned.1.call-start = ((), (), s32[]{:S(2)}) async-start(), calls=%async_computation.8 | async-start | bytes 3194880 | tf_op jit(solution)/shard_map/all_gather | solution.py:62
  27.6 84.2 %all-to-all-start = ((bf16[8,32,2048]{2,1,0:T(8,128)(2,1)}), bf16[8,32,2048]{2,1,0:T(8,128)(2,1)S(1)}, u32[]{:S(2)}, u32[]{:S(2)}) async-start(bf16[8,32,2048]{2,1,0:T(8,128)(2,1)} %broadcast_in_dim.15), calls=%async_computation | async-start | bytes 2097152 | tf_op jit(solution)/shard_map/all_to_all | solution.py:20
  158.3 72.1 %copy-start.7 = (f32[768]{0:T(1024)S(1)}, f32[768]{0:T(1024)}, u32[]{:S(2)}) copy-start(f32[768]{0:T(1024)} %param.27) | copy-start | bytes 9220
  235.4 28.9 %copy-start = (bf16[32,2048]{1,0:T(8,128)(2,1)S(1)}, bf16[32,2048]{1,0:T(8,128)(2,1)}, u32[]{:S(2)}) copy-start(bf16[32,2048]{1,0:T(8,128)(2,1)} %param.20) | copy-start | bytes 393220
  235.4 29.0 %copy-start.2 = (f32[2048]{0:T(1024)S(1)}, f32[2048]{0:T(1024)}, u32[]{:S(2)}) copy-start(f32[2048]{0:T(1024)} %param.22) | copy-start | bytes 24580
  264.1 6.0 %copy-start.1 = (f32[256,32]{0,1:T(8,128)S(1)}, f32[256,32]{0,1:T(8,128)}, u32[]{:S(2)}) copy-start(f32[256,32]{0,1:T(8,128)} %param.36) | copy-start | bytes 98308
  264.1 109.4 %copy-start.8 = (f32[256]{0:T(256)S(1)}, f32[256]{0:T(256)}, u32[]{:S(2)}) copy-start(f32[256]{0:T(256)} %param.33) | copy-start | bytes 3076
  264.6 110.7 %copy-start.9 = (f32[256]{0:T(256)S(1)}, f32[256]{0:T(256)}, u32[]{:S(2)}) copy-start(f32[256]{0:T(256)} %param.31) | copy-start | bytes 3076
  265.7 107.9 %all-to-all-start.2 = ((bf16[8,32,2048]{2,1,0:T(8,128)(2,1)}), bf16[8,32,2048]{2,1,0:T(8,128)(2,1)S(1)}, u32[]{:S(2)}, u32[]{:S(2)}) async-start(bf16[8,32,2048]{2,1,0:T(8,128)(2,1)} %broadcast_in_dim.16), calls=%async_computation.2 | async-start | bytes 2097152 | tf_op jit(solution)/shard_map/all_to_all | solution.py:20
  270.2 169.6 %all-gather.12.cloned.1.call-start = ((), (), s32[]{:S(2)}) async-start(), calls=%async_computation.9 | async-start | bytes 1114112 | tf_op jit(solution)/shard_map/all_gather | solution.py:72
  280.9 96.5 %copy-start.10 = (f32[256]{0:T(256)S(1)}, f32[256]{0:T(256)}, u32[]{:S(2)}) copy-start(f32[256]{0:T(256)} %param.35) | copy-start | bytes 3076
  381.8 90.0 %copy-start.3 = (f32[2048]{0:T(1024)S(1)}, f32[2048]{0:T(1024)}, u32[]{:S(2)}) copy-start(f32[2048]{0:T(1024)} %param.23) | copy-start | bytes 24580
Sparse Core Ops, SparseCore 0:
  10.3 147.9 all-gather.5
  160.4 69.9 all-gather.7
  233.3 140.1 all-gather.9
  375.5 64.2 all-gather.11
where the time goes:
time: 525 us; the launch traced here: 524 us
  waiting for transfers between devices  266 us (51%)
  blocking collectives  190 us (36%)
  matrix products  24.4 us (5%)
  starting transfers between devices  16.4 us (3%)
  between operations  13.5 us (3%)
  other arithmetic  11.2 us (2%)
    all_gather x2, waiting for transfers between devices, side_by_side(): whole, at, done = (lax.all_gather(both, axis, axis=dim, tiled=True), 0, [])  139 us
    all_gather x2, waiting for transfers between devices, gather_axes(): whole = lax.all_gather(whole, axes[number], axis=dim, tiled=True)  127 us
    all_to_all x3, blocking collectives, sent_and_summed(): lax.all_to_all(pieces, axis, split_axis=0, concat_axis=0, tiled=True)  77.1 us
    all_gather x1, blocking collectives, gather_turned(): whole = lax.all_gather(both, axis, axis=0, tiled=True)  72.2 us
    all_gather x2, blocking collectives, gather_axes(): whole = lax.all_gather(whole, axes[number], axis=dim, tiled=True)  21.9 us
    all_to_all x1, blocking collectives, sent_to_all(): lax.all_to_all(jnp.broadcast_to(x[None], (peers, *x.shape)), axis, 0, 0,...  18.4 us
    all_to_all x2, starting transfers between devices, sent_to_all(): lax.all_to_all(jnp.broadcast_to(x[None], (peers, *x.shape)), axis, 0, 0,...  16.3 us
    dot_general x3, matrix products, return_rows(): term = jnp.dot(inputs, weight, preferred_element_type=jnp.float32) * factor  11.7 us
  transfers between devices with their start and end apart: 6, of which 4 were waited for; matrix products, arithmetic and copies ran while one was open for 5% of the time, Pallas kernels for 0%

commit v1 on v0

--- a/solution.py
+++ b/solution.py
@@ -15,6 +15,13 @@
 HIGHEST = lax.Precision.HIGHEST
 
 
+def gather_over(shard, name, d):
+    peers = lax.axis_size(name)
+    blocks = jnp.stack([shard for _ in range(peers)])
+    blocks = lax.all_to_all(blocks, name, split_axis=0, concat_axis=0)
+    return jnp.concatenate(blocks, axis=d)
+
+
 def sent_to_all(x, axis):
     peers = lax.axis_size(axis)
     return lax.all_to_all(jnp.broadcast_to(x[None], (peers, *x.shape)), axis, 0, 0, tiled=True)
@@ -47,7 +54,7 @@
     turned = [jnp.moveaxis(a, dim, 0) for a, dim in zip(arrays, dims)]
     widths = [t[0].size for t in turned]
     both = jnp.concatenate([t.reshape(-1, w) for t, w in zip(turned, widths)], axis=1)
-    whole = lax.all_gather(both, axis, axis=0, tiled=True)
+    whole = gather_over(both, axis, 0)
     pieces = jnp.split(whole, [sum(widths[:k]) for k in range(1, len(widths))], axis=1)
     return tuple(
         (

time: 525 us -> 525 us (level)
  blocking collectives: 190 us -> 117 us
  waiting for transfers between devices: 266 us -> 322 us
  starting transfers between devices: 16.4 us -> 31.5 us
    all_gather x1 -> x0, blocking collectives: 72.2 us -> none  [gather_turned(): whole = lax.all_gather(both, axis, axis=0, tiled=True)]
    all_gather x2, waiting for transfers between devices: 139 us -> 168 us  [side_by_side(): whole, at, done = (lax.all_gather(both, axis, axis=dim, tiled=True), 0, [])]
    all_to_all x0 -> x1, starting transfers between devices: none -> 17.8 us  [gather_over(): blocks = lax.all_to_all(blocks, name, split_axis=0, concat_axis=0)]
    all_to_all x2, waiting for transfers between devices: 0.01 us -> 14.8 us  [sent_to_all(): lax.all_to_all(jnp.broadcast_to(x[None], (peers, *x.shape)), axis, 0, 0,...]
    all_to_all x0 -> x1, waiting for transfers between devices: none -> 12.6 us  [gather_over(): blocks = lax.all_to_all(blocks, name, split_axis=0, concat_axis=0)]
  transfers between devices with their start and end apart: 6 -> 7, of which waited for: 4 -> 6; matrix products, arithmetic and copies ran while one was open for 5% -> 5% of each run, Pallas kernels for 0% -> 0%
where the time goes in v1:
time: 525 us; the launch traced here: 524 us
  waiting for transfers between devices  322 us (61%)
  blocking collectives  117 us (22%)
  starting transfers between devices  31.5 us (6%)
  matrix products  24.4 us (5%)
  between operations  13.5 us (3%)
  other arithmetic  11.8 us (2%)
    all_gather x2, waiting for transfers between devices, side_by_side(): whole, at, done = (lax.all_gather(both, axis, axis=dim, tiled=True), 0, [])  168 us
    all_gather x2, waiting for transfers between devices, gather_axes(): whole = lax.all_gather(whole, axes[number], axis=dim, tiled=True)  127 us
    all_to_all x3, blocking collectives, sent_and_summed(): lax.all_to_all(pieces, axis, split_axis=0, concat_axis=0, tiled=True)  77.1 us
    all_gather x2, blocking collectives, gather_axes(): whole = lax.all_gather(whole, axes[number], axis=dim, tiled=True)  21.9 us
    all_to_all x1, blocking collectives, sent_to_all(): lax.all_to_all(jnp.broadcast_to(x[None], (peers, *x.shape)), axis, 0, 0,...  18.4 us
    all_to_all x1, starting transfers between devices, gather_over(): blocks = lax.all_to_all(blocks, name, split_axis=0, concat_axis=0)  17.8 us
    all_to_all x2, waiting for transfers between devices, sent_to_all(): lax.all_to_all(jnp.broadcast_to(x[None], (peers, *x.shape)), axis, 0, 0,...  14.8 us
    all_to_all x2, starting transfers between devices, sent_to_all(): lax.all_to_all(jnp.broadcast_to(x[None], (peers, *x.shape)), axis, 0, 0,...  13.7 us
  transfers between devices with their start and end apart: 7, of which 6 were waited for; matrix products, arithmetic and copies ran while one was open for 5% of the time, Pallas kernels for 0%

profile of v1, /device:TPU:1, one launch (start us, length us, event | category | flops | bytes accessed | tf_op | source)
XLA Modules:
  0.0 524.3 jit_solution(15250793743828293477)
XLA Ops:
  10.0 11.3 %all_gather.19 = bf16[768,128]{0,1:T(8,128)(2,1)} all-gather(bf16[768,32]{0,1:T(8,128)(2,1)S(1)} %convert_element_type.133), channel_id=1, replica_groups=mesh['fs_0'=16,'fs_1'=4,'tp'=8] {'fs_1'}, dimensions={1}, use_global_device_ids=true | all-gather | bytes 245760 | tf_op jit(solution)/shard_map/all_gather | solution.py:79
  25.6 17.8 %all-to-all-start.1 = ((f32[64,32,2]{1,2,0:T(2,128)}), f32[64,32,2]{1,2,0:T(2,128)S(1)}, u32[]{:S(2)}, u32[]{:S(2)}) async-start(f32[64,32,2]{1,2,0:T(2,128)} %stack.2), calls=%async_computation.1 | async-start | bytes 131072 | tf_op jit(solution)/shard_map/all_to_all | solution.py:21
  45.4 12.6 %all-to-all-done.1 = f32[64,32,2]{1,2,0:T(2,128)S(1)} async-done(((f32[64,32,2]{1,2,0:T(2,128)}), f32[64,32,2]{1,2,0:T(2,128)S(1)}, u32[]{:S(2)}, u32[]{:S(2)}) %all-to-all-start.1) | async-done | bytes 16416 | tf_op jit(solution)/shard_map/all_to_all | solution.py:21
  58.1 1.2 broadcast_in_dim.15
  59.3 9.2 %all-to-all-start = ((bf16[8,32,2048]{2,1,0:T(8,128)(2,1)}), bf16[8,32,2048]{2,1,0:T(8,128)(2,1)S(1)}, u32[]{:S(2)}, u32[]{:S(2)}) async-start(bf16[8,32,2048]{2,1,0:T(8,128)(2,1)} %broadcast_in_dim.15), calls=%async_computation | async-start | bytes 2097152 | tf_op jit(solution)/shard_map/all_to_all | solution.py:27
  68.6 14.8 %all-to-all-done = bf16[8,32,2048]{2,1,0:T(8,128)(2,1)S(1)} async-done(((bf16[8,32,2048]{2,1,0:T(8,128)(2,1)}), bf16[8,32,2048]{2,1,0:T(8,128)(2,1)S(1)}, u32[]{:S(2)}, u32[]{:S(2)}) %all-to-all-start) | async-done | bytes 1048608 | tf_op jit(solution)/shard_map/all_to_all | solution.py:27
  83.4 75.1 %all-gather.5.cloned.1.call-done = bf16[2048,1536]{1,0:T(8,128)(2,1)} async-done(((bf16[32,1536]{1,0:T(8,128)(2,1)}), bf16[2048,1536]{1,0:T(8,128)(2,1)}) %all-gather.5.cloned.1.call-update) | async-done | bytes 6291472 | tf_op jit(solution)/shard_map/all_gather | solution.py:69
  158.5 2.9 fusion.11
  161.4 69.1 %all-gather.7.cloned.1.call-done = bf16[768,2048]{0,1:T(8,128)(2,1)} async-done(((bf16[768,128]{0,1:T(8,128)(2,1)}), bf16[768,2048]{0,1:T(8,128)(2,1)}) %all-gather.7.cloned.1.call-update) | async-done | bytes 3145744 | tf_op jit(solution)/shard_map/all_gather | solution.py:79
  230.5 5.0 fusion.8
  235.6 28.7 %all_to_all.35 = bf16[8,32,2048]{2,1,0:T(8,128)(2,1)S(1)} all-to-all(bf16[8,32,2048]{2,1,0:T(8,128)(2,1)S(1)} %bitcast.73), channel_id=1, replica_groups=mesh['fs_0'=16,'fs_1'=4,'tp'=8] {'tp'}, dimensions={0} | all-to-all | bytes 2097152 | tf_op jit(solution)/shard_map/all_to_all | solution.py:49
  265.8 4.5 all-to-all-start.3
  270.3 10.6 %all_gather.22 = bf16[256,128]{0,1:T(8,128)(2,1)} all-gather(bf16[256,32]{0,1:T(8,128)(2,1)S(1)} %convert_element_type.148), channel_id=1, replica_groups=mesh['fs_0'=16,'fs_1'=4,'tp'=8] {'fs_1'}, dimensions={1}, use_global_device_ids=true | all-gather | bytes 81920 | tf_op jit(solution)/shard_map/all_gather | solution.py:79
  281.2 92.5 %all-gather.9.cloned.1.call-done = bf16[2048,768]{1,0:T(8,128)(2,1)} async-done(((bf16[32,768]{1,0:T(8,128)(2,1)}), bf16[2048,768]{1,0:T(8,128)(2,1)}) %all-gather.9.cloned.1.call-update) | async-done | bytes 3145744 | tf_op jit(solution)/shard_map/all_gather | solution.py:69
  373.7 1.7 fusion.35
  375.4 1.7 fusion.36
  377.7 1.7 fusion.37
  382.0 58.0 %all-gather.11.cloned.1.call-done = bf16[256,2048]{0,1:T(8,128)(2,1)} async-done(((bf16[256,128]{0,1:T(8,128)(2,1)}), bf16[256,2048]{0,1:T(8,128)(2,1)}) %all-gather.11.cloned.1.call-update) | async-done | bytes 1048592 | tf_op jit(solution)/shard_map/all_gather | solution.py:79
  440.0 1.7 fusion.10
  441.7 30.0 %all_to_all.36 = bf16[8,32,2048]{2,1,0:T(8,128)(2,1)S(1)} all-to-all(bf16[8,32,2048]{2,1,0:T(8,128)(2,1)S(1)} %bitcast.64), channel_id=1, replica_groups=mesh['fs_0'=16,'fs_1'=4,'tp'=8] {'tp'}, dimensions={0} | all-to-all | bytes 2097152 | tf_op jit(solution)/shard_map/all_to_all | solution.py:49
  472.2 18.4 %all_to_all.37 = bf16[8,32,2048]{2,1,0:T(8,128)(2,1)S(1)} all-to-all(bf16[8,32,2048]{2,1,0:T(8,128)(2,1)S(1)} %broadcast_in_dim.19), channel_id=1, replica_groups=mesh['fs_0'=16,'fs_1'=4,'tp'=8] {'tp'}, dimensions={0} | all-to-all | bytes 2097152 | tf_op jit(solution)/shard_map/all_to_all | solution.py:27
  490.6 2.9 fusion.14
  493.5 5.0 fusion.9
  498.5 18.4 %all_to_all.38 = bf16[8,32,2048]{2,1,0:T(8,128)(2,1)S(1)} all-to-all(bf16[8,32,2048]{2,1,0:T(8,128)(2,1)S(1)} %bitcast.72), channel_id=1, replica_groups=mesh['fs_0'=16,'fs_1'=4,'tp'=8] {'tp'}, dimensions={0} | all-to-all | bytes 2097152 | tf_op jit(solution)/shard_map/all_to_all | solution.py:49
  (78 shorter events, 16.5 us)
Async XLA Ops:
  6.5 151.9 %copy-start.4 = (f32[768]{0:T(1024)S(1)}, f32[768]{0:T(1024)}, u32[]{:S(2)}) copy-start(f32[768]{0:T(1024)} %param.25) | copy-start | bytes 9220
  6.5 151.9 %all-gather.5.cloned.1.call-start = ((), (), s32[]{:S(2)}) async-start(), calls=%async_computation.7 | async-start | bytes 6389760 | tf_op jit(solution)/shard_map/all_gather | solution.py:69
  9.0 221.5 %all-gather.7.cloned.1.call-start = ((), (), s32[]{:S(2)}) async-start(), calls=%async_computation.8 | async-start | bytes 3342336 | tf_op jit(solution)/shard_map/all_gather | solution.py:79
  21.3 352.4 %all-gather.9.cloned.1.call-start = ((), (), s32[]{:S(2)}) async-start(), calls=%async_computation.9 | async-start | bytes 3194880 | tf_op jit(solution)/shard_map/all_gather | solution.py:69
  25.6 32.5 %all-to-all-start.1 = ((f32[64,32,2]{1,2,0:T(2,128)}), f32[64,32,2]{1,2,0:T(2,128)S(1)}, u32[]{:S(2)}, u32[]{:S(2)}) async-start(f32[64,32,2]{1,2,0:T(2,128)} %stack.2), calls=%async_computation.1 | async-start | bytes 131072 | tf_op jit(solution)/shard_map/all_to_all | solution.py:21
  59.3 24.1 %all-to-all-start = ((bf16[8,32,2048]{2,1,0:T(8,128)(2,1)}), bf16[8,32,2048]{2,1,0:T(8,128)(2,1)S(1)}, u32[]{:S(2)}, u32[]{:S(2)}) async-start(bf16[8,32,2048]{2,1,0:T(8,128)(2,1)} %broadcast_in_dim.15), calls=%async_computation | async-start | bytes 2097152 | tf_op jit(solution)/shard_map/all_to_all | solution.py:27
  158.5 72.1 %copy-start.5 = (f32[768]{0:T(1024)S(1)}, f32[768]{0:T(1024)}, u32[]{:S(2)}) copy-start(f32[768]{0:T(1024)} %param.27) | copy-start | bytes 9220
  235.6 28.9 %copy-start = (bf16[32,2048]{1,0:T(8,128)(2,1)S(1)}, bf16[32,2048]{1,0:T(8,128)(2,1)}, u32[]{:S(2)}) copy-start(bf16[32,2048]{1,0:T(8,128)(2,1)} %param.20) | copy-start | bytes 393220
  235.6 29.0 %copy-start.2 = (f32[2048]{0:T(1024)S(1)}, f32[2048]{0:T(1024)}, u32[]{:S(2)}) copy-start(f32[2048]{0:T(1024)} %param.22) | copy-start | bytes 24580
  264.3 6.0 %copy-start.1 = (f32[256,32]{0,1:T(8,128)S(1)}, f32[256,32]{0,1:T(8,128)}, u32[]{:S(2)}) copy-start(f32[256,32]{0,1:T(8,128)} %param.36) | copy-start | bytes 98308
  264.3 109.4 %copy-start.6 = (f32[256]{0:T(256)S(1)}, f32[256]{0:T(256)}, u32[]{:S(2)}) copy-start(f32[256]{0:T(256)} %param.33) | copy-start | bytes 3076
  264.7 110.7 %copy-start.7 = (f32[256]{0:T(256)S(1)}, f32[256]{0:T(256)}, u32[]{:S(2)}) copy-start(f32[256]{0:T(256)} %param.31) | copy-start | bytes 3076
  265.8 107.9 %all-to-all-start.3 = ((bf16[8,32,2048]{2,1,0:T(8,128)(2,1)}), bf16[8,32,2048]{2,1,0:T(8,128)(2,1)S(1)}, u32[]{:S(2)}, u32[]{:S(2)}) async-start(bf16[8,32,2048]{2,1,0:T(8,128)(2,1)} %broadcast_in_dim.16), calls=%async_computation.3 | async-start | bytes 2097152 | tf_op jit(solution)/shard_map/all_to_all | solution.py:27
  270.3 169.6 %all-gather.11.cloned.1.call-start = ((), (), s32[]{:S(2)}) async-start(), calls=%async_computation.10 | async-start | bytes 1114112 | tf_op jit(solution)/shard_map/all_gather | solution.py:79
  281.1 96.5 %copy-start.8 = (f32[256]{0:T(256)S(1)}, f32[256]{0:T(256)}, u32[]{:S(2)}) copy-start(f32[256]{0:T(256)} %param.35) | copy-start | bytes 3076
  382.0 90.0 %copy-start.3 = (f32[2048]{0:T(1024)S(1)}, f32[2048]{0:T(1024)}, u32[]{:S(2)}) copy-start(f32[2048]{0:T(1024)} %param.23) | copy-start | bytes 24580
Sparse Core Ops, SparseCore 0:
  10.3 148.1 all-gather.4
  160.6 69.9 all-gather.6
  233.5 140.1 all-gather.8
  375.6 64.2 all-gather.10
